TPU v7x, 32 devices: a whole 2x2x4 slice. The times are simulated.
32 devices in a mesh: grp: 2 (over y), sp: 4 (over z), tp: 4 (over x, core).
Axes of the slice: x: 2, y: 2, z: 4, core: 2. Of those that a mesh axis runs over, the one named last changes fastest.
Arguments:
- tokens: bfloat16 [8, 1024, 4096], P(('grp', 'tp'), 'sp'), parts along dimension 0, may hold values from -8 to 8, as said below
- offsets: int32 [8], P(('grp', 'tp')), parts along dimension 0, may hold values from 0 to 4095
- in_gain: float32 [4096], replicated, may hold values from 0.1 to 1.9
- w_latent: bfloat16 [4096, 1024], P('sp'), may hold values from -0.09375 to 0.09375
- w_rope_key: bfloat16 [4096, 32], replicated, may hold values from -0.09375 to 0.09375
- kv_gain: float32 [1024], replicated, may hold values from 0.1 to 1.9
- w_up_key: bfloat16 [1024, 2048], P(None, 'tp'), may hold values from -0.1875 to 0.1875
- w_up_value: bfloat16 [1024, 2048], P(None, 'tp'), may hold values from -0.1875 to 0.1875
- q_nope: bfloat16 [8, 2048], P(('grp', 'sp'), 'tp'), parts along dimension 0, may hold values from -300 to 300, as said below
- q_rope: bfloat16 [8, 1024], P(('grp', 'sp'), 'tp'), parts along dimension 0, may hold values from -16 to 16
Outputs:
- keys: bfloat16 [8, 1024, 2048], P(('grp', 'sp'), None, 'tp'), parts along dimension 0
- values: bfloat16 [8, 1024, 2048], P(('grp', 'sp'), None, 'tp'), parts along dimension 0
- rope_keys: bfloat16 [8, 32, 1024], P(('grp', 'sp')), parts along dimension 0
- read: bfloat16 [8, 2048], P(('grp', 'sp'), 'tp'), parts along dimension 0
There are 2 independent parts, one for each index of `grp`. A program takes and returns all parts, laid end to end along the dimension named above; an argument that names none is the same for every part. Nothing has to cross between parts.
Inputs may be any that keep to these rules, and one draw needn't show every extreme that they name: `tokens`: entries of the layer's input. `q_nope`: entries of the first decoding token's queries.
All inputs are finite; a program needn't handle non-finite values.
Results may differ from a plain program's by a relative error of at most 0.02.
Values may be sent and summed in bfloat16 or wider, within the bound.
A program may use at most 128 MiB of HBM per device.

v0:
```python
import jax
import jax.numpy as jnp
from jax import lax
from jax.sharding import PartitionSpec as P

HEAD = 64
ROPE = 32


EPS = 1e-06


def rms_scale(values, gain):
    wide = values.astype(jnp.float32)
    return wide * lax.rsqrt(jnp.mean(wide * wide, axis=-1, keepdims=True) + EPS) * gain


def rotate(raw, position):
    inverse = 10000.0 ** (-jnp.arange(0, ROPE, 2).astype(jnp.float32) / ROPE)
    angle = position.astype(jnp.float32)[..., None] * inverse
    cosine, sine = (jnp.cos(angle), jnp.sin(angle))
    half = ROPE // 2
    first, second = (raw[..., :half], raw[..., half:])
    return jnp.concatenate(
        [first * cosine - second * sine, second * cosine + first * sine], axis=-1
    )


def local(
    tokens, offsets, in_gain, w_latent, w_rope_key, kv_gain, w_up_key, w_up_value, q_nope, q_rope
):
    prompts, rows, width = tokens.shape
    n_sp = lax.axis_size("sp")
    length = n_sp * rows
    block = lax.axis_index("sp")
    normed = rms_scale(tokens.reshape(prompts * rows, width), in_gain).astype(jnp.bfloat16)
    latent_raw = jnp.dot(
        normed,
        lax.all_gather(w_latent, "sp", axis=0, tiled=True),
        preferred_element_type=jnp.float32,
    )
    latent = rms_scale(latent_raw, kv_gain).astype(jnp.bfloat16)
    position = offsets[:, None] + block * rows + jnp.arange(rows, dtype=jnp.int32)[None, :]
    rope_raw = jnp.dot(normed, w_rope_key, preferred_element_type=jnp.float32).reshape(
        prompts, rows, ROPE
    )
    rotated = rotate(rope_raw, position).astype(jnp.bfloat16)
    head_cols = w_up_key.shape[1]
    latent_every, rope_every = (
        lax.all_gather(latent.reshape(prompts, rows, latent.shape[1]), "tp", axis=0, tiled=True),
        lax.all_gather(rotated, "tp", axis=0, tiled=True),
    )
    latent_moved, rope_moved = (
        lax.all_to_all(latent_every[:, None], "sp", split_axis=0, concat_axis=1, tiled=True),
        lax.all_to_all(rope_every[:, None], "sp", split_axis=0, concat_axis=1, tiled=True),
    )
    latent_all = latent_moved.reshape(length, latent_moved.shape[3])
    rope_all = rope_moved.reshape(length, ROPE)
    keys = jnp.dot(latent_all, w_up_key, preferred_element_type=jnp.float32).astype(jnp.bfloat16)
    values = jnp.dot(latent_all, w_up_value, preferred_element_type=jnp.float32).astype(
        jnp.bfloat16
    )
    rope_keys = rope_all.T
    heads_here = head_cols // HEAD
    query = q_nope.reshape(heads_here, HEAD)
    rotary_q = q_rope.reshape(heads_here, ROPE)
    keys_split = keys.reshape(length, heads_here, HEAD)
    scores = jnp.einsum("hd,jhd->hj", query, keys_split, preferred_element_type=jnp.float32)
    scores = scores + jnp.dot(rotary_q, rope_keys, preferred_element_type=jnp.float32)
    scores = scores / jnp.sqrt(jnp.float32(HEAD + ROPE))
    peak = jnp.max(scores, axis=-1, keepdims=True)
    expo = jnp.exp(scores - peak)
    weights = (expo / jnp.sum(expo, axis=-1, keepdims=True)).astype(jnp.bfloat16)
    read = jnp.einsum(
        "hj,jhd->hd",
        weights,
        values.reshape(length, heads_here, HEAD),
        preferred_element_type=jnp.float32,
    )
    read = read.astype(jnp.bfloat16).reshape(1, heads_here * HEAD)
    return (keys[None], values[None], rope_keys[None], read)


def solution(mesh):
    in_specs = (
        P(("grp", "tp"), "sp", None),
        P(("grp", "tp")),
        P(),
        P("sp", None),
        P(),
        P(),
        P(None, "tp"),
        P(None, "tp"),
        P(("grp", "sp"), "tp"),
        P(("grp", "sp"), "tp"),
    )
    out_specs = (
        P(("grp", "sp"), None, "tp"),
        P(("grp", "sp"), None, "tp"),
        P(("grp", "sp"), None, None),
        P(("grp", "sp"), "tp"),
    )
    return jax.shard_map(local, mesh=mesh, in_specs=in_specs, out_specs=out_specs, check_vma=False)
```

profile of v0, /device:TPU:3, one launch (start us, length us, event | category | flops | bytes accessed | tf_op | source)
XLA Modules:
  0.0 256.9 jit_solution(4544893987934630213)
XLA Ops:
  7.2 0.7 all-gather.4.cloned.1.call-update
  8.0 0.9 copy-done.1
  8.9 0.5 fusion
  9.4 151.2 %all-gather.4.cloned.1.call-done = bf16[4096,1024]{1,0:T(8,128)(2,1)} async-done(((bf16[1024,1024]{1,0:T(8,128)(2,1)}), bf16[4096,1024]{1,0:T(8,128)(2,1)}) %all-gather.4.cloned.1.call-update) | async-done | bytes 8388624 | tf_op jit(solution)/shard_map/all_gather | solution.py:39
  160.6 5.9 %multiply_reduce_fusion = (f32[256]{0:T(256)S(1)}, f32[256,1024]{1,0:T(8,128)S(1)}) fusion(bf16[4096,1024]{1,0:T(8,128)(2,1)} %all-gather.4.cloned.1.call-done, bf16[1,256,4096]{2,1,0:T(8,128)(2,1)S(1)} %copy-done.1, f32[4096]{0:T(1024)S(1)} %copy-done.10, f32[256]{0:T(256)S(1)} %add_rsqrt_fusion.1), kind=kOutput, calls=%fused_computation.12 | convolution fusion | flops 2152201984 | bytes 11552768 | tf_op jit(solution)/shard_map/dot_general | solution.py:37
  166.5 0.9 multiply_convert_fusion
  168.2 0.8 convolution_bitcast_fusion.1
  168.9 0.2 fusion.16
  169.1 5.6 %all_gather.11 = bf16[4,256,32]{1,2,0:T(8,128)(2,1)S(1)} all-gather(bf16[1,256,32]{1,2,0:T(8,128)(2,1)S(1)} %pad_maximum_fusion), channel_id=1, replica_groups=mesh['grp'=2,'sp'=4,'tp'=4] {'tp'}, dimensions={0}, use_global_device_ids=true | all-gather | bytes 81920 | tf_op jit(solution)/shard_map/all_gather | solution.py:51
  174.7 7.0 %all_to_all.8 = bf16[4,1,256,32]{2,3,1,0:T(8,128)(2,1)S(1)} all-to-all(bf16[4,1,256,32]{2,3,1,0:T(8,128)(2,1)S(1)} %bitcast.64), channel_id=1, replica_groups=mesh['grp'=2,'sp'=4,'tp'=4] {'sp'}, dimensions={0} | all-to-all | bytes 131072 | tf_op jit(solution)/shard_map/all_to_all | solution.py:55
  181.7 5.8 %all-gather.6.cloned.1.call-done = bf16[1024,1024]{1,0:T(8,128)(2,1)} async-done(((bf16[256,1024]{1,0:T(8,128)(2,1)}), bf16[1024,1024]{1,0:T(8,128)(2,1)}) %all-gather.6.cloned.1.call-update) | async-done | bytes 2097168 | tf_op jit(solution)/shard_map/all_gather | solution.py:50
  187.5 4.7 %all-to-all-start = ((bf16[4,1,256,1024]{3,2,1,0:T(8,128)(2,1)}), bf16[4,1,256,1024]{3,2,1,0:T(8,128)(2,1)S(1)}, u32[]{:S(2)}, u32[]{:S(2)}) async-start(bf16[4,1,256,1024]{3,2,1,0:T(8,128)(2,1)} %bitcast.59), calls=%async_computation | async-start | bytes 4194304 | tf_op jit(solution)/shard_map/all_to_all | solution.py:54
  192.5 47.4 %all-to-all-done = bf16[4,1,256,1024]{3,2,1,0:T(8,128)(2,1)S(1)} async-done(((bf16[4,1,256,1024]{3,2,1,0:T(8,128)(2,1)}), bf16[4,1,256,1024]{3,2,1,0:T(8,128)(2,1)S(1)}, u32[]{:S(2)}, u32[]{:S(2)}) %all-to-all-start) | async-done | bytes 2097184 | tf_op jit(solution)/shard_map/all_to_all | solution.py:54
  239.9 1.3 copy-done.2
  241.2 3.0 %convolution_convert_fusion.1 = bf16[1024,512]{0,1:T(8,128)(2,1)S(1)} fusion(bf16[1024,1024]{1,0:T(8,128)(2,1)} %bitcast.60, bf16[1024,512]{1,0:T(8,128)(2,1)S(1)} %copy-done), kind=kOutput, calls=%fused_computation.6 | convolution fusion | flops 1074266112 | bytes 4194304 | tf_op jit(solution)/shard_map/dot_general | solution.py:59
  244.3 0.2 fusion.21
  244.5 0.2 fusion.20
  244.8 0.2 fusion.10
  245.0 0.1 fusion.19
  245.1 1.3 convolution_convert_fusion
  246.4 0.4 fusion.8
  246.8 0.7 reshape.216
  247.5 1.3 copy.22
  248.8 1.3 copy.23
  (35 shorter events, 0.5 us)
Async XLA Ops:
  7.2 234.1 %copy-start = (bf16[1024,512]{1,0:T(8,128)(2,1)S(1)}, bf16[1024,512]{1,0:T(8,128)(2,1)}, u32[]{:S(2)}) copy-start(bf16[1024,512]{1,0:T(8,128)(2,1)} %param.16) | copy-start | bytes 3145732
  7.2 1.7 copy-start.1
  7.2 153.4 %copy-start.10 = (f32[4096]{0:T(1024)S(1)}, f32[4096]{0:T(1024)}, u32[]{:S(2)}) copy-start(f32[4096]{0:T(1024)} %param.12) | copy-start | bytes 49156
  7.2 153.4 %all-gather.4.cloned.1.call-start = ((), (), s32[]{:S(2)}) async-start(), calls=%async_computation.2 | async-start | bytes 10485760 | tf_op jit(solution)/shard_map/all_gather | solution.py:39
  7.9 179.5 %all-gather.6.cloned.1.call-start = ((), (), s32[]{:S(2)}) async-start(), calls=%async_computation.3 | async-start | bytes 2621440 | tf_op jit(solution)/shard_map/all_gather | solution.py:50
  9.4 157.1 %copy-start.5 = (f32[1024]{0:T(1024)S(1)}, f32[1024]{0:T(1024)}, u32[]{:S(2)}) copy-start(f32[1024]{0:T(1024)} %param.15) | copy-start | bytes 12292
  166.5 1.7 copy-start.9
  187.5 4.7 %copy-start.6 = (bf16[1,512]{1,0:T(2,128)(2,1)S(1)}, bf16[1,512]{1,0:T(2,128)(2,1)}, u32[]{:S(2)}) copy-start(bf16[1,512]{1,0:T(2,128)(2,1)} %param.18) | copy-start | bytes 3076
  187.5 4.8 %copy-start.7 = (bf16[1,256]{1,0:T(2,128)(2,1)S(1)}, bf16[1,256]{1,0:T(2,128)(2,1)}, u32[]{:S(2)}) copy-start(bf16[1,256]{1,0:T(2,128)(2,1)} %param.19) | copy-start | bytes 1540
  187.5 52.4 %all-to-all-start = ((bf16[4,1,256,1024]{3,2,1,0:T(8,128)(2,1)}), bf16[4,1,256,1024]{3,2,1,0:T(8,128)(2,1)S(1)}, u32[]{:S(2)}, u32[]{:S(2)}) async-start(bf16[4,1,256,1024]{3,2,1,0:T(8,128)(2,1)} %bitcast.59), calls=%async_computation | async-start | bytes 4194304 | tf_op jit(solution)/shard_map/all_to_all | solution.py:54
  192.4 54.0 %copy-start.4 = (bf16[4,8,4,256]{3,1,2,0:T(8,128)(2,1)}, bf16[4,8,4,256]{3,1,2,0:T(8,128)(2,1)S(1)}, u32[]{:S(2)}) copy-start(bf16[4,8,4,256]{3,1,2,0:T(8,128)(2,1)S(1)} %copy.28) | copy-start | bytes 196612
  239.9 1.3 copy-start.2
  241.2 3.8 %copy-start.3 = (bf16[4,1,256,1024]{3,2,1,0:T(8,128)(2,1)S(1)}, bf16[4,1,256,1024]{3,2,1,0:T(8,128)(2,1)}, u32[]{:S(2)}) copy-start(bf16[4,1,256,1024]{3,2,1,0:T(8,128)(2,1)} %copy-done.2) | copy-start | bytes 6291460
  241.2 3.8 %copy-start.8 = (bf16[1024,512]{1,0:T(8,128)(2,1)S(1)}, bf16[1024,512]{1,0:T(8,128)(2,1)}, u32[]{:S(2)}) copy-start(bf16[1024,512]{1,0:T(8,128)(2,1)} %param.17) | copy-start | bytes 3145732
Sparse Core Ops, SparseCore 0:
  9.6 150.9 all-gather.3
  167.6 19.8 all-gather.5
where the time goes:
time: 260 us; the launch traced here: 257 us
  waiting for transfers between devices  205 us (79%)
  between operations  14.9 us (6%)
  blocking collectives  12.6 us (5%)
  matrix products  11.8 us (5%)
  local copies, waits for them, and re-layouts  5.8 us (2%)
  starting transfers between devices  4.73 us (2%)
    all_gather x1, waiting for transfers between devices, local(): lax.all_gather(w_latent, 'sp', axis=0, tiled=True)  151 us
    all_to_all x1, waiting for transfers between devices, local(): lax.all_to_all(latent_every[:, None], 'sp', split_axis=0, concat_axis=1,...  47.4 us
    all_to_all x1, blocking collectives, local(): lax.all_to_all(rope_every[:, None], 'sp', split_axis=0, concat_axis=1, ti...  7.02 us
    dot_general x1, matrix products, local(): jnp.dot(normed, lax.all_gather(w_latent, 'sp', axis=0, tiled=True), prefe...  5.85 us
    all_gather x1, waiting for transfers between devices, local(): lax.all_gather(latent.reshape(prompts, rows, latent.shape[1]), 'tp', axis...  5.76 us
    all_gather x1, blocking collectives, local(): lax.all_gather(rotated, 'tp', axis=0, tiled=True)  5.58 us
  transfers between devices with their start and end apart: 3, of which 3 were waited for; matrix products, arithmetic and copies ran while one was open for 1% of the time, Pallas kernels for 0%

commit v1 on v0

v1 whole, which is shorter than its diff:
```python
import functools

import jax
import jax.numpy as jnp
from jax import lax
from jax.experimental import pallas as pl
from jax.experimental.pallas import tpu as pltpu
from jax.sharding import PartitionSpec as P

HEAD = 64
ROPE = 32
LANES = 128
CORES = 2


EPS = 1e-06
MESH = pl.DeviceIdType.MESH


def gather_kernel(
    n_grp,
    n_sp,
    n_tp,
    groups,
    tok_hbm,
    w_hbm,
    w_rope,
    in_gain,
    cosine,
    sine,
    lat_out,
    rope_out,
    tok,
    w_own,
    normed,
    wbuf,
    acc,
    own,
    own_rope,
    transit,
    local_sem,
    z_send,
    z_recv,
    a_send,
    a_recv,
    b_send,
    b_recv,
    c_send,
    c_recv,
    l_send,
    t_send,
    t_recv,
    x_send,
    d_send,
    l_recv,
):
    n_x = n_tp // CORES
    prompts, rows = own.shape[1:3]
    depth, cols = w_own.shape
    width = cols // groups
    chunk = wbuf.shape[5]
    y, z, t = lax.axis_index("grp"), lax.axis_index("sp"), lax.axis_index("tp")
    x, core = t // CORES, t % CORES
    rank = (core * n_x + x) * n_grp + y
    half = n_x // 2

    def tp_of(x_to, core_to):
        return {"tp": x_to * CORES + core_to}

    x_peers = [lax.rem(x + k, n_x) for k in range(1, n_x)]
    y_peers = [lax.rem(y + k, n_grp) for k in range(1, n_grp)]
    z_peers = [lax.rem(z + k, n_sp) for k in range(1, n_sp)]

    fetch_tok = pltpu.make_async_copy(tok_hbm, tok, local_sem.at[0])
    fetch_w = pltpu.make_async_copy(w_hbm, w_own, local_sem.at[1])
    fetch_tok.start()
    fetch_w.start()

    barrier = pltpu.get_barrier_semaphore()
    targets = (
        [tp_of(p, core) for p in x_peers]
        + [{"grp": p} for p in y_peers]
        + [{"sp": p} for p in z_peers]
        + [tp_of(x, 1 - core)]
    )
    for target in targets:
        pl.semaphore_signal(barrier, inc=1, device_id=target, device_id_type=MESH)
    pl.semaphore_wait(barrier, len(targets))

    finish = []

    def remote(src, dst, send, recv, device):
        return pltpu.make_async_remote_copy(
            src_ref=src,
            dst_ref=dst,
            send_sem=send,
            recv_sem=recv,
            device_id=device,
            device_id_type=MESH,
        )

    def arrived(ref, recv):
        remote(ref, ref, recv, recv, tp_of(x, 1 - core)).wait_recv()

    units = [(g, d) for g in range(groups) for d in range(1, n_sp)]

    def stage_z(u):
        g, d = units[u]
        copy = remote(
            w_hbm.at[pl.ds(rank * chunk, chunk), pl.ds(g * width, width)],
            wbuf.at[g, d - 1, core, x, y],
            z_send.at[u],
            z_recv.at[u],
            {"sp": lax.rem(z + n_sp - d, n_sp)},
        )
        copy.start()
        finish.append(copy.wait_send)

    def x_first(g):
        return g % 2 == 1

    def spread(u, src, send, recv, along_x):
        peers = x_peers if along_x else y_peers
        for k, peer in enumerate(peers):
            copy = remote(
                src,
                src,
                send.at[u, k],
                recv.at[u, k],
                tp_of(peer, core) if along_x else {"grp": peer},
            )
            copy.start()
            finish.append(copy.wait_send)

    def block_a(u):
        g, d = units[u]
        return wbuf.at[g, d - 1, core, x, y]

    def block_b(u):
        g, d = units[u]
        if x_first(g):
            return wbuf.at[g, d - 1, core, :, y]
        return wbuf.at[g, d - 1, core, x]

    def stage_a(u):
        arrived(block_a(u), z_recv.at[u])
        spread(u, block_a(u), a_send, a_recv, x_first(units[u][0]))

    def stage_b(u):
        g, _ = units[u]
        for k in range(len(x_peers if x_first(g) else y_peers)):
            arrived(block_a(u), a_recv.at[u, k])
        spread(u, block_b(u), b_send, b_recv, not x_first(g))

    def stage_c(u):
        g, d = units[u]
        for k in range(len(y_peers if x_first(g) else x_peers)):
            arrived(block_b(u), b_recv.at[u, k])
        ref = wbuf.at[g, d - 1, core]
        copy = remote(ref, ref, c_send.at[u], c_recv.at[u], tp_of(x, 1 - core))
        copy.start()
        finish.append(copy.wait_send)

    def stage_dot(u):
        g, d = units[u]
        arrived(wbuf.at[g, d - 1, core], c_recv.at[u])
        weight = wbuf[g, d - 1].reshape(depth, width)
        acc[g] += jnp.dot(
            normed[lax.rem(z + d, n_sp)], weight, preferred_element_type=jnp.float32
        )

    def crossing(m):
        return m % 2 == 0 and m > 0 and m < groups and n_x % 2 == 0

    def slot(m, s):
        if m == 0:
            return rope_out.at[s]
        return lat_out.at[s, :, pl.ds((m - 1) * width, width)]

    def mine(m, i):
        return own_rope.at[i] if m == 0 else own.at[m - 1, i]

    swapped = lax.rem(x + half, n_x) * CORES + core

    def stage_l(m):
        for i in range(prompts):
            home = t * prompts + i
            if crossing(m):
                copy = remote(
                    mine(m, i), transit.at[m, i], l_send.at[m, i], t_recv.at[m, i], {"tp": swapped}
                )
            else:
                copy = remote(
                    mine(m, i), slot(m, z), l_send.at[m, i], l_recv.at[m, z], {"sp": home}
                )
            pl.when(home != z)(copy.start)
            finish.append(lambda home=home, copy=copy: pl.when(home != z)(copy.wait_send))

    def stage_t(m):
        for i in range(prompts):
            home = swapped * prompts + i
            copy = remote(
                transit.at[m, i], slot(m, z), t_send.at[m, i], l_recv.at[m, z], {"sp": home}
            )

            def pass_on(m=m, i=i, copy=copy):
                arrived(transit.at[m, i], t_recv.at[m, i])
                copy.start()

            pl.when(home != z)(pass_on)
            finish.append(lambda home=home, copy=copy: pl.when(home != z)(copy.wait_send))

    owner = z // prompts

    def entry(m, e):
        x_in, core_in = owner // CORES, owner % CORES
        if crossing(m) and e > 0:
            x_in = lax.rem(x_in + half, n_x)
        return x_in, core_in

    def partner_copy(m, e):
        s = lax.rem(z + e, n_sp)
        return remote(slot(m, s), slot(m, s), d_send.at[m, e], l_recv.at[m, s], tp_of(x, 1 - core))

    def stage_x(m, e):
        s = lax.rem(z + e, n_sp)
        x_in, core_in = entry(m, e)
        here = (x == x_in) & (core == core_in)
        copies = [
            remote(slot(m, s), slot(m, s), x_send.at[m, e, k], l_recv.at[m, s], tp_of(peer, core))
            for k, peer in enumerate(x_peers)
        ]

        def enter():
            if e > 0:
                arrived(slot(m, s), l_recv.at[m, s])
            for copy in copies:
                copy.start()
            partner_copy(m, e).start()

        pl.when(here)(enter)

        def drain():
            for copy in copies:
                copy.wait_send()
            partner_copy(m, e).wait_send()

        finish.append(lambda: pl.when(here)(drain))

    def stage_d(m, e):
        s = lax.rem(z + e, n_sp)
        x_in, core_in = entry(m, e)
        here = (x != x_in) & (core == core_in)

        def hand():
            arrived(slot(m, s), l_recv.at[m, s])
            partner_copy(m, e).start()

        pl.when(here)(hand)
        finish.append(lambda: pl.when(here)(partner_copy(m, e).wait_send))

    def stage_end(m, e):
        s = lax.rem(z + e, n_sp)
        _, core_in = entry(m, e)
        pl.when(core != core_in)(lambda: arrived(slot(m, s), l_recv.at[m, s]))

    def finalize(m, value):
        value = value.reshape(prompts, rows, value.shape[-1])
        for i in range(prompts):
            mine(m, i)[...] = value[i]

            def keep(i=i):
                slot(m, z)[...] = value[i]

            pl.when(t * prompts + i == z)(keep)

    for u in range(len(units)):
        stage_z(u)

    fetch_tok.wait()
    step_rows = 16

    def norm(r, carry):
        at = pl.ds(pl.multiple_of(r * step_rows, step_rows), step_rows)
        wide = tok[at, :].astype(jnp.float32)
        scale = lax.rsqrt(jnp.mean(wide * wide, axis=-1, keepdims=True) + EPS)
        out = (wide * scale * in_gain[...]).astype(jnp.bfloat16)
        for b in range(n_sp):
            normed[b, at, :] = out[:, b * depth : (b + 1) * depth]
        return carry

    lax.fori_loop(0, prompts * rows // step_rows, norm, 0)

    work = {}

    def at_step(step, fn, *args):
        work.setdefault(step, []).append((fn, args))

    def own_dot(g):
        acc[g] = jnp.dot(
            normed[z], w_own[:, g * width : (g + 1) * width], preferred_element_type=jnp.float32
        )

    def rope_item():
        raw = jnp.dot(normed[0], w_rope[:depth, :], preferred_element_type=jnp.float32)
        for b in range(1, n_sp):
            raw += jnp.dot(
                normed[b], w_rope[b * depth : (b + 1) * depth, :], preferred_element_type=jnp.float32
            )
        other = pltpu.roll(raw, LANES - ROPE, 1)
        finalize(0, (raw * cosine[...] + other * sine[...]).astype(jnp.bfloat16))

    def group_item(g):
        finalize(g + 1, acc[g].astype(jnp.bfloat16))

    def route(m, step):
        at_step(step, stage_l, m)
        if crossing(m):
            at_step(step + 2, stage_t, m)
            step += 2
        for e in range(n_sp):
            at_step(step + 2, stage_x, m, e)
        for e in range(n_sp):
            at_step(step + 4, stage_d, m, e)

    lag_b, lag_c, lag_dot = 2, 4, 5
    for u, (g, d) in enumerate(units):
        at_step(u, stage_a, u)
        at_step(u + lag_b, stage_b, u)
        at_step(u + lag_c, stage_c, u)
    at_step(0, fetch_w.wait)
    for g in range(groups):
        at_step(g + 1, own_dot, g)
    at_step(1, rope_item)
    for u, (g, d) in enumerate(units):
        at_step(max(u + lag_dot, g + 1), stage_dot, u)
        if d == n_sp - 1:
            at_step(max(u + lag_dot, g + 1), group_item, g)
    route(0, 2)
    for g in range(groups):
        route(g + 1, max((g + 1) * (n_sp - 1) - 1 + lag_dot, g + 1))

    for step in sorted(work):
        for fn, args in work[step]:
            fn(*args)
    for m in range(groups + 1):
        for e in range(n_sp):
            stage_end(m, e)
    for fn in finish:
        fn()


def gather_latent(tokens, w_latent, w_rope, in_gain, cosine, sine):
    prompts, rows, width = tokens.shape
    n_grp, n_sp, n_tp = (lax.axis_size(a) for a in ("grp", "sp", "tp"))
    n_x = n_tp // CORES
    depth, cols = w_latent.shape
    groups = max(1, 16 // n_sp // 4 * 4) if n_sp <= 4 else 1
    part = cols // groups
    chunk = depth // (n_grp * n_tp)
    total = prompts * rows
    units = groups * (n_sp - 1)
    peers = max(n_x, n_grp) - 1
    items = groups + 1
    bf16, f32 = jnp.bfloat16, jnp.float32
    dma = pltpu.SemaphoreType.DMA
    vmem = pl.BlockSpec(memory_space=pltpu.VMEM)
    hbm = pl.BlockSpec(memory_space=pl.ANY)
    return pl.pallas_call(
        functools.partial(gather_kernel, n_grp, n_sp, n_tp, groups),
        out_shape=(
            jax.ShapeDtypeStruct((n_sp, rows, cols), bf16),
            jax.ShapeDtypeStruct((n_sp, rows, LANES), bf16),
        ),
        in_specs=[hbm, hbm, vmem, vmem, vmem, vmem],
        out_specs=(vmem, vmem),
        scratch_shapes=[
            pltpu.VMEM((total, width), bf16),
            pltpu.VMEM((depth, cols), bf16),
            pltpu.VMEM((n_sp, total, depth), bf16),
            pltpu.VMEM((groups, n_sp - 1, CORES, n_x, n_grp, chunk, part), bf16),
            pltpu.VMEM((groups, total, part), f32),
            pltpu.VMEM((groups, prompts, rows, part), bf16),
            pltpu.VMEM((prompts, rows, LANES), bf16),
            pltpu.VMEM((items, prompts, rows, part), bf16),
            dma((2,)),
            dma((units,)),
            dma((units,)),
            dma((units, peers)),
            dma((units, peers)),
            dma((units, peers)),
            dma((units, peers)),
            dma((units,)),
            dma((units,)),
            dma((items, prompts)),
            dma((items, prompts)),
            dma((items, prompts)),
            dma((items, n_sp, max(n_x - 1, 1))),
            dma((items, n_sp)),
            dma((items, n_sp)),
        ],
        compiler_params=pltpu.CompilerParams(
            collective_id=0, has_side_effects=True, vmem_limit_bytes=60 * 1024 * 1024
        ),
    )(tokens.reshape(total, width), w_latent, w_rope, in_gain, cosine, sine)


def cache_kernel(
    n_blocks,
    latent_ref,
    gain_ref,
    wk_ref,
    wv_ref,
    query_ref,
    rope_q_ref,
    rope_ref,
    keys_ref,
    values_ref,
    read_ref,
    scores,
    held,
):
    b = pl.program_id(0)
    rows = latent_ref.shape[1]
    raw = latent_ref[0].astype(jnp.float32)
    scale = lax.rsqrt(jnp.mean(raw * raw, axis=-1, keepdims=True) + EPS)
    latent = (raw * scale * gain_ref[...]).astype(jnp.bfloat16)
    keys = jnp.dot(latent, wk_ref[...], preferred_element_type=jnp.float32).astype(jnp.bfloat16)
    keys_ref[...] = keys
    values = jnp.dot(latent, wv_ref[...], preferred_element_type=jnp.float32).astype(jnp.bfloat16)
    values_ref[...] = values
    held[b] = values
    across = (((1,), (1,)), ((), ()))
    part = lax.dot_general(query_ref[...], keys, across, preferred_element_type=jnp.float32)
    part += lax.dot_general(
        rope_q_ref[...], rope_ref[0], across, preferred_element_type=jnp.float32
    )
    scores[b] = part / jnp.sqrt(jnp.float32(HEAD + ROPE))

    @pl.when(b == n_blocks - 1)
    def _():
        every = scores[...]
        peak = jnp.max(jnp.max(every, axis=-1, keepdims=True), axis=0, keepdims=True)
        expo = jnp.exp(every - peak)
        total = jnp.sum(jnp.sum(expo, axis=-1, keepdims=True), axis=0, keepdims=True)
        weights = (expo / total).astype(jnp.bfloat16)
        out = jnp.dot(weights[0], held[0], preferred_element_type=jnp.float32)
        for i in range(1, n_blocks):
            out += jnp.dot(weights[i], held[i], preferred_element_type=jnp.float32)
        head = lax.broadcasted_iota(jnp.int32, out.shape, 0)
        lane = lax.broadcasted_iota(jnp.int32, out.shape, 1)
        picked = jnp.where((lane >= head * HEAD) & (lane < head * HEAD + HEAD), out, 0.0)
        read_ref[...] = jnp.sum(picked, axis=0, keepdims=True).astype(jnp.bfloat16)


def fill_cache(latent, kv_gain, w_up_key, w_up_value, query, rotary_q, rope):
    n_blocks, rows, cols = latent.shape
    out_cols = w_up_key.shape[1]
    heads = query.shape[0]
    length = n_blocks * rows
    whole = lambda shape: pl.BlockSpec(shape, lambda b: (0,) * len(shape))
    return pl.pallas_call(
        functools.partial(cache_kernel, n_blocks),
        grid=(n_blocks,),
        out_shape=(
            jax.ShapeDtypeStruct((length, out_cols), jnp.bfloat16),
            jax.ShapeDtypeStruct((length, out_cols), jnp.bfloat16),
            jax.ShapeDtypeStruct((1, out_cols), jnp.bfloat16),
        ),
        in_specs=[
            pl.BlockSpec((1, rows, cols), lambda b: (b, 0, 0)),
            whole((1, cols)),
            whole((cols, out_cols)),
            whole((cols, out_cols)),
            whole(query.shape),
            whole(rotary_q.shape),
            pl.BlockSpec((1, rows, LANES), lambda b: (b, 0, 0)),
        ],
        out_specs=(
            pl.BlockSpec((rows, out_cols), lambda b: (b, 0)),
            pl.BlockSpec((rows, out_cols), lambda b: (b, 0)),
            whole((1, out_cols)),
        ),
        scratch_shapes=[
            pltpu.VMEM((n_blocks, heads, rows), jnp.float32),
            pltpu.VMEM((n_blocks, rows, out_cols), jnp.bfloat16),
        ],
    )(latent, kv_gain, w_up_key, w_up_value, query, rotary_q, rope)


def local(
    tokens, offsets, in_gain, w_latent, w_rope_key, kv_gain, w_up_key, w_up_value, q_nope, q_rope
):
    prompts, rows, _ = tokens.shape
    block = lax.axis_index("sp")
    half = ROPE // 2
    position = offsets[:, None] + block * rows + jnp.arange(rows, dtype=jnp.int32)[None, :]
    inverse = 10000.0 ** (-jnp.arange(0, ROPE, 2).astype(jnp.float32) / ROPE)
    angle = position.reshape(-1).astype(jnp.float32)[:, None] * inverse
    pad = ((0, 0), (0, LANES - ROPE))
    cosine, sine = jnp.cos(angle), jnp.sin(angle)
    cosine = jnp.pad(jnp.concatenate([cosine, cosine], axis=1), pad)
    sine = jnp.pad(jnp.concatenate([-sine, sine], axis=1), pad)
    w_rope = jnp.concatenate([w_rope_key, w_rope_key[:, half:], w_rope_key[:, :half]], axis=1)
    w_rope = jnp.pad(w_rope, ((0, 0), (0, LANES - 2 * ROPE)))
    latent, rope = gather_latent(tokens, w_latent, w_rope, in_gain[None], cosine, sine)

    heads = w_up_key.shape[1] // HEAD
    eye = jnp.eye(heads, dtype=q_nope.dtype)
    query = (eye[:, :, None] * q_nope.reshape(1, heads, HEAD)).reshape(heads, heads * HEAD)
    rotary_q = jnp.pad(q_rope.reshape(heads, ROPE), pad)
    keys, values, read = fill_cache(
        latent, kv_gain[None], w_up_key, w_up_value, query, rotary_q, rope
    )
    rope_keys = rope.reshape(-1, LANES)[:, :ROPE].T
    return (keys[None], values[None], rope_keys[None], read)


def solution(mesh):
    in_specs = (
        P(("grp", "tp"), "sp", None),
        P(("grp", "tp")),
        P(),
        P("sp", None),
        P(),
        P(),
        P(None, "tp"),
        P(None, "tp"),
        P(("grp", "sp"), "tp"),
        P(("grp", "sp"), "tp"),
    )
    out_specs = (
        P(("grp", "sp"), None, "tp"),
        P(("grp", "sp"), None, "tp"),
        P(("grp", "sp"), None, None),
        P(("grp", "sp"), "tp"),
    )
    return jax.shard_map(local, mesh=mesh, in_specs=in_specs, out_specs=out_specs, check_vma=False)
```

time: 260 us -> 106 us (0.41); the launches traced: 257 us -> 106 us
  waiting for transfers between devices: 205 us -> 0 us
  Pallas kernels: 0 us -> 94.4 us
  between operations: 14.9 us -> 1.4 us
  blocking collectives: 12.6 us -> 0 us
  matrix products: 11.8 us -> 0 us
  starting transfers between devices: 4.73 us -> 0 us
    all_gather x2 -> x0, waiting for transfers between devices: 157 us -> none  [the longest x1 151 us: local(): lax.all_gather(w_latent, 'sp', axis=0, tiled=True)]
    pallas_call x0 -> x2, Pallas kernels: none -> 94.4 us  [the longest x1 87.3 us: gather_latent(): pl.pallas_call(functools.partial(gather_kernel, n_grp, n_sp, n_tp, groups...]
    all_to_all x1 -> x0, waiting for transfers between devices: 47.4 us -> none  [local(): lax.all_to_all(latent_every[:, None], 'sp', split_axis=0, concat_axis=1,...]
    dot_general x7 -> x0, matrix products: 11.8 us -> none  [the longest x1 5.85 us: local(): jnp.dot(normed, lax.all_gather(w_latent, 'sp', axis=0, tiled=True), prefe...]
    all_to_all x1 -> x0, blocking collectives: 7.02 us -> none  [local(): lax.all_to_all(rope_every[:, None], 'sp', split_axis=0, concat_axis=1, ti...]
    all_gather x1 -> x0, blocking collectives: 5.58 us -> none  [local(): lax.all_gather(rotated, 'tp', axis=0, tiled=True)]
    all_to_all x1 -> x0, starting transfers between devices: 4.66 us -> none  [local(): lax.all_to_all(latent_every[:, None], 'sp', split_axis=0, concat_axis=1,...]
    unnamed x25 -> x6, local copies, waits for them, and re-layouts: 4.89 us -> 1.24 us
  transfers between devices with their start and end apart: 3 -> 0, of which waited for: 3 -> 0; matrix products, arithmetic and copies ran while one was open for 1% -> 0% of each run, Pallas kernels for 0% -> 0%
where the time goes in v1:
time: 106 us
  Pallas kernels  94.4 us (89%)
  local copies, waits for them, and re-layouts  5.54 us (5%)
  other arithmetic  4.31 us (4%)
  between operations  1.4 us (1%)
    pallas_call x1, Pallas kernels, gather_latent(): pl.pallas_call(functools.partial(gather_kernel, n_grp, n_sp, n_tp, groups...  87.3 us
    pallas_call x1, Pallas kernels, fill_cache(): pl.pallas_call(functools.partial(cache_kernel, n_blocks), grid=(n_blocks,...  7.02 us
    concatenate x1, other arithmetic, local(): jnp.concatenate([w_rope_key, w_rope_key[:, half:], w_rope_key[:, :half]],...  2.13 us

profile of v1, /device:TPU:3, one launch (start us, length us, event | category | flops | bytes accessed | tf_op | source)
XLA Modules:
  0.0 105.6 jit_solution(7883972206144779222)
XLA Ops:
  0.6 0.0 copy-start.1
  1.3 0.7 reduce.1
  2.1 0.7 reduce
  2.8 0.1 reshape.51
  2.8 0.6 pad.18.rope_q_ref
  3.4 0.1 mul.46
  3.5 0.1 mul.47
  3.6 0.6 broadcast_multiply_fusion.query_ref
  4.2 0.1 fusion.5
  4.4 0.1 copy.21
  4.5 0.7 pad.16.cosine
  5.1 0.1 copy.22
  5.2 0.7 pad.17.sine
  5.9 1.0 fusion.7
  6.9 0.5 copy.19
  7.4 0.5 copy.20
  7.8 0.0 copy-done.1
  7.9 0.5 copy.18
  8.3 2.1 %fusion.4.w_rope = bf16[4096,128]{1,0:T(8,128)(2,1)} fusion(bf16[4096,16]{1,0:T(8,128)(2,1)S(1)} %copy.20, bf16[4096,16]{1,0:T(8,128)(2,1)S(1)} %copy.19, bf16[4096,32]{1,0:T(8,128)(2,1)S(1)} %copy.18), kind=kLoop, calls=%fused_computation.5 | loop fusion | flops 5242880 | bytes 1572864 | tf_op jit(solution)/shard_map/concatenate | solution.py:504
  10.5 87.3 %shard_map.129 = (bf16[4,256,1024]{2,1,0:T(8,128)(2,1)}, bf16[4,256,128]{2,1,0:T(8,128)(2,1)}) custom-call(bf16[256,4096]{1,0:T(8,128)(2,1)} %bitcast.14, bf16[1024,1024]{1,0:T(8,128)(2,1)} %w_hbm.1, bf16[4096,128]{1,0:T(8,128)(2,1)} %fusion.4.w_rope, f32[1,4096]{1,0:T(1,128)} %bitcast.17, f32[256,128]{1,0:T(8,128)} %pad.16.cosine, f32[256,128]{1,0:T(8,128)} %pad.17.sine), custom_call_target="tpu_custom_call" | custom-call | tf_op jit(solution)/shard_map/pallas_call | solution.py:369
  97.8 0.0 copy-start
  97.8 7.0 %shard_map.130 = (bf16[1024,512]{1,0:T(8,128)(2,1)}, bf16[1024,512]{1,0:T(8,128)(2,1)}, bf16[1,512]{1,0:T(2,128)(2,1)}) custom-call(bf16[4,256,1024]{2,1,0:T(8,128)(2,1)} %get-tuple-element.9.latent_ref, f32[1,1024]{1,0:T(1,128)} %bitcast.18, bf16[1024,512]{1,0:T(8,128)(2,1)} %wk_ref.1, bf16[1024,512]{1,0:T(8,128)(2,1)} %wv_ref.1, ...), custom_call_target="tpu_custom_call" | custom-call | tf_op jit(solution)/shard_map/pallas_call | solution.py:462
  104.8 0.0 copy-done
  104.9 0.8 copy.24
  (4 shorter events, 0.0 us)
Async XLA Ops:
  0.6 7.2 %copy-start.1 = (bf16[4096,32]{0,1:T(8,128)(2,1)S(1)}, bf16[4096,32]{0,1:T(8,128)(2,1)}, u32[]{:S(2)}) copy-start(bf16[4096,32]{0,1:T(8,128)(2,1)} %param.14) | copy-start | bytes 786436
  97.8 7.0 %copy-start = (bf16[4,256,128]{2,1,0:T(8,128)(2,1)S(1)}, bf16[4,256,128]{2,1,0:T(8,128)(2,1)}, u32[]{:S(2)}) copy-start(bf16[4,256,128]{2,1,0:T(8,128)(2,1)} %get-tuple-element.10.rope_ref) | copy-start | bytes 786436

commit v2 on v1

--- a/solution.py
+++ b/solution.py
@@ -2,6 +2,7 @@
 
 import jax
 import jax.numpy as jnp
+import numpy as np
 from jax import lax
 from jax.experimental import pallas as pl
 from jax.experimental.pallas import tpu as pltpu
@@ -11,6 +12,9 @@
 ROPE = 32
 LANES = 128
 CORES = 2
+GROUPS = 4
+LAGS = (3, 6, 7)
+HOP = 3
 
 
 EPS = 1e-06
@@ -24,14 +28,15 @@
     groups,
     tok_hbm,
     w_hbm,
-    w_rope,
+    w_rope_hbm,
     in_gain,
-    cosine,
-    sine,
+    offsets,
+    inverse,
     lat_out,
     rope_out,
     tok,
     w_own,
+    w_rope,
     normed,
     wbuf,
     acc,
@@ -73,8 +78,10 @@
 
     fetch_tok = pltpu.make_async_copy(tok_hbm, tok, local_sem.at[0])
     fetch_w = pltpu.make_async_copy(w_hbm, w_own, local_sem.at[1])
+    fetch_rope = pltpu.make_async_copy(w_rope_hbm, w_rope, local_sem.at[2])
     fetch_tok.start()
     fetch_w.start()
+    fetch_rope.start()
 
     barrier = pltpu.get_barrier_semaphore()
     targets = (
@@ -116,8 +123,8 @@
         copy.start()
         finish.append(copy.wait_send)
 
-    def x_first(g):
-        return g % 2 == 1
+    def x_first(u):
+        return u % 2 == 1
 
     def spread(u, src, send, recv, along_x):
         peers = x_peers if along_x else y_peers
@@ -138,23 +145,23 @@
 
     def block_b(u):
         g, d = units[u]
-        if x_first(g):
+        if x_first(u):
             return wbuf.at[g, d - 1, core, :, y]
         return wbuf.at[g, d - 1, core, x]
 
     def stage_a(u):
         arrived(block_a(u), z_recv.at[u])
-        spread(u, block_a(u), a_send, a_recv, x_first(units[u][0]))
+        spread(u, block_a(u), a_send, a_recv, x_first(u))
 
     def stage_b(u):
         g, _ = units[u]
-        for k in range(len(x_peers if x_first(g) else y_peers)):
+        for k in range(len(x_peers if x_first(u) else y_peers)):
             arrived(block_a(u), a_recv.at[u, k])
-        spread(u, block_b(u), b_send, b_recv, not x_first(g))
+        spread(u, block_b(u), b_send, b_recv, not x_first(u))
 
     def stage_c(u):
         g, d = units[u]
-        for k in range(len(y_peers if x_first(g) else x_peers)):
+        for k in range(len(y_peers if x_first(u) else x_peers)):
             arrived(block_b(u), b_recv.at[u, k])
         ref = wbuf.at[g, d - 1, core]
         copy = remote(ref, ref, c_send.at[u], c_recv.at[u], tp_of(x, 1 - core))
@@ -277,8 +284,7 @@
     for u in range(len(units)):
         stage_z(u)
 
-    fetch_tok.wait()
-    step_rows = 16
+    step_rows, pieces = 16, 4
 
     def norm(r, carry):
         at = pl.ds(pl.multiple_of(r * step_rows, step_rows), step_rows)
@@ -289,7 +295,9 @@
             normed[b, at, :] = out[:, b * depth : (b + 1) * depth]
         return carry
 
-    lax.fori_loop(0, prompts * rows // step_rows, norm, 0)
+    def norm_piece(k):
+        turns = prompts * rows // step_rows // pieces
+        lax.fori_loop(k * turns, (k + 1) * turns, norm, 0)
 
     work = {}
 
@@ -302,13 +310,30 @@
         )
 
     def rope_item():
-        raw = jnp.dot(normed[0], w_rope[:depth, :], preferred_element_type=jnp.float32)
-        for b in range(1, n_sp):
-            raw += jnp.dot(
-                normed[b], w_rope[b * depth : (b + 1) * depth, :], preferred_element_type=jnp.float32
+        fetch_rope.wait()
+        raw = jnp.zeros((prompts * rows, ROPE), jnp.float32)
+        for b in range(n_sp):
+            raw += lax.dot_general(
+                normed[b],
+                w_rope[:, b * depth : (b + 1) * depth],
+                (((1,), (1,)), ((), ())),
+                preferred_element_type=jnp.float32,
             )
-        other = pltpu.roll(raw, LANES - ROPE, 1)
-        finalize(0, (raw * cosine[...] + other * sine[...]).astype(jnp.bfloat16))
+        half_rope = ROPE // 2
+        blank = jnp.zeros((prompts * rows, LANES - ROPE), jnp.float32)
+        lane = lax.broadcasted_iota(jnp.int32, (rows, LANES), 1)
+        index = lax.broadcasted_iota(jnp.int32, (rows, LANES), 0)
+        plain = jnp.concatenate([raw, blank], axis=1)
+        other = jnp.concatenate([raw[:, half_rope:], raw[:, :half_rope], blank], axis=1)
+        turned = []
+        for i in range(prompts):
+            position = offsets[i] + z * rows + index
+            angle = position.astype(jnp.float32) * inverse[...]
+            sine = jnp.sin(angle)
+            sine = jnp.where(lane < half_rope, -sine, sine)
+            at = slice(i * rows, (i + 1) * rows)
+            turned.append(plain[at] * jnp.cos(angle) + other[at] * sine)
+        finalize(0, jnp.concatenate(turned, axis=0).astype(jnp.bfloat16))
 
     def group_item(g):
         finalize(g + 1, acc[g].astype(jnp.bfloat16))
@@ -316,29 +341,32 @@
     def route(m, step):
         at_step(step, stage_l, m)
         if crossing(m):
-            at_step(step + 2, stage_t, m)
-            step += 2
+            step += HOP
+            at_step(step, stage_t, m)
         for e in range(n_sp):
-            at_step(step + 2, stage_x, m, e)
+            at_step(step + HOP, stage_x, m, e)
         for e in range(n_sp):
-            at_step(step + 4, stage_d, m, e)
-
-    lag_b, lag_c, lag_dot = 2, 4, 5
+            at_step(step + 2 * HOP, stage_d, m, e)
+
+    lag_b, lag_c, lag_dot = LAGS
     for u, (g, d) in enumerate(units):
         at_step(u, stage_a, u)
         at_step(u + lag_b, stage_b, u)
         at_step(u + lag_c, stage_c, u)
-    at_step(0, fetch_w.wait)
-    for g in range(groups):
-        at_step(g + 1, own_dot, g)
-    at_step(1, rope_item)
+    at_step(0, fetch_tok.wait)
+    for k in range(pieces):
+        at_step(k, norm_piece, k)
+    at_step(pieces, fetch_w.wait)
+    at_step(pieces, rope_item)
+    route(0, pieces)
     for u, (g, d) in enumerate(units):
-        at_step(max(u + lag_dot, g + 1), stage_dot, u)
+        step = max(u + lag_dot, pieces)
+        if d == 1:
+            at_step(step, own_dot, g)
+        at_step(step, stage_dot, u)
         if d == n_sp - 1:
-            at_step(max(u + lag_dot, g + 1), group_item, g)
-    route(0, 2)
-    for g in range(groups):
-        route(g + 1, max((g + 1) * (n_sp - 1) - 1 + lag_dot, g + 1))
+            at_step(step, group_item, g)
+            route(g + 1, step)
 
     for step in sorted(work):
         for fn, args in work[step]:
@@ -350,12 +378,12 @@
         fn()
 
 
-def gather_latent(tokens, w_latent, w_rope, in_gain, cosine, sine):
+def gather_latent(tokens, w_latent, w_rope, in_gain, offsets, inverse):
     prompts, rows, width = tokens.shape
     n_grp, n_sp, n_tp = (lax.axis_size(a) for a in ("grp", "sp", "tp"))
     n_x = n_tp // CORES
     depth, cols = w_latent.shape
-    groups = max(1, 16 // n_sp // 4 * 4) if n_sp <= 4 else 1
+    groups = max(1, GROUPS * 3 // (n_sp - 1) // 4 * 4)
     part = cols // groups
     chunk = depth // (n_grp * n_tp)
     total = prompts * rows
@@ -372,18 +400,19 @@
             jax.ShapeDtypeStruct((n_sp, rows, cols), bf16),
             jax.ShapeDtypeStruct((n_sp, rows, LANES), bf16),
         ),
-        in_specs=[hbm, hbm, vmem, vmem, vmem, vmem],
+        in_specs=[hbm, hbm, hbm, vmem, pl.BlockSpec(memory_space=pltpu.SMEM), vmem],
         out_specs=(vmem, vmem),
         scratch_shapes=[
             pltpu.VMEM((total, width), bf16),
             pltpu.VMEM((depth, cols), bf16),
+            pltpu.VMEM((ROPE, width), bf16),
             pltpu.VMEM((n_sp, total, depth), bf16),
             pltpu.VMEM((groups, n_sp - 1, CORES, n_x, n_grp, chunk, part), bf16),
             pltpu.VMEM((groups, total, part), f32),
             pltpu.VMEM((groups, prompts, rows, part), bf16),
             pltpu.VMEM((prompts, rows, LANES), bf16),
             pltpu.VMEM((items, prompts, rows, part), bf16),
-            dma((2,)),
+            dma((3,)),
             dma((units,)),
             dma((units,)),
             dma((units, peers)),
@@ -402,7 +431,7 @@
         compiler_params=pltpu.CompilerParams(
             collective_id=0, has_side_effects=True, vmem_limit_bytes=60 * 1024 * 1024
         ),
-    )(tokens.reshape(total, width), w_latent, w_rope, in_gain, cosine, sine)
+    )(tokens.reshape(total, width), w_latent, w_rope, in_gain, offsets, inverse)
 
 
 def cache_kernel(
@@ -411,17 +440,35 @@
     gain_ref,
     wk_ref,
     wv_ref,
-    query_ref,
-    rope_q_ref,
+    q_nope_ref,
+    q_rope_ref,
     rope_ref,
     keys_ref,
     values_ref,
+    rope_keys_ref,
     read_ref,
     scores,
     held,
 ):
     b = pl.program_id(0)
-    rows = latent_ref.shape[1]
+    heads = scores.shape[1]
+
+    def per_head(row, size):
+        wide = jnp.broadcast_to(row.astype(jnp.float32), (heads, heads * size))
+        head = lax.broadcasted_iota(jnp.int32, wide.shape, 0)
+        lane = lax.broadcasted_iota(jnp.int32, wide.shape, 1)
+        return jnp.where((lane >= head * size) & (lane < head * size + size), wide, 0.0)
+
+    query = per_head(q_nope_ref[...], HEAD).astype(jnp.bfloat16)
+    spread = (heads * ROPE, LANES)
+    fold = lax.broadcasted_iota(jnp.int32, spread, 0) % ROPE == lax.broadcasted_iota(
+        jnp.int32, spread, 1
+    )
+    rotary_q = jnp.dot(
+        per_head(q_rope_ref[...], ROPE).astype(jnp.bfloat16),
+        jnp.where(fold, 1.0, 0.0).astype(jnp.bfloat16),
+        preferred_element_type=jnp.float32,
+    ).astype(jnp.bfloat16)
     raw = latent_ref[0].astype(jnp.float32)
     scale = lax.rsqrt(jnp.mean(raw * raw, axis=-1, keepdims=True) + EPS)
     latent = (raw * scale * gain_ref[...]).astype(jnp.bfloat16)
@@ -430,11 +477,11 @@
     values = jnp.dot(latent, wv_ref[...], preferred_element_type=jnp.float32).astype(jnp.bfloat16)
     values_ref[...] = values
     held[b] = values
+    rope = rope_ref[0]
+    rope_keys_ref[...] = rope.astype(jnp.float32).T[:ROPE].astype(jnp.bfloat16)
     across = (((1,), (1,)), ((), ()))
-    part = lax.dot_general(query_ref[...], keys, across, preferred_element_type=jnp.float32)
-    part += lax.dot_general(
-        rope_q_ref[...], rope_ref[0], across, preferred_element_type=jnp.float32
-    )
+    part = lax.dot_general(query, keys, across, preferred_element_type=jnp.float32)
+    part += lax.dot_general(rotary_q, rope, across, preferred_element_type=jnp.float32)
     scores[b] = part / jnp.sqrt(jnp.float32(HEAD + ROPE))
 
     @pl.when(b == n_blocks - 1)
@@ -453,10 +500,10 @@
         read_ref[...] = jnp.sum(picked, axis=0, keepdims=True).astype(jnp.bfloat16)
 
 
-def fill_cache(latent, kv_gain, w_up_key, w_up_value, query, rotary_q, rope):
+def fill_cache(latent, kv_gain, w_up_key, w_up_value, q_nope, q_rope, rope):
     n_blocks, rows, cols = latent.shape
     out_cols = w_up_key.shape[1]
-    heads = query.shape[0]
+    heads = out_cols // HEAD
     length = n_blocks * rows
     whole = lambda shape: pl.BlockSpec(shape, lambda b: (0,) * len(shape))
     return pl.pallas_call(
@@ -465,6 +512,7 @@
         out_shape=(
             jax.ShapeDtypeStruct((length, out_cols), jnp.bfloat16),
             jax.ShapeDtypeStruct((length, out_cols), jnp.bfloat16),
+            jax.ShapeDtypeStruct((ROPE, length), jnp.bfloat16),
             jax.ShapeDtypeStruct((1, out_cols), jnp.bfloat16),
         ),
         in_specs=[
@@ -472,47 +520,34 @@
             whole((1, cols)),
             whole((cols, out_cols)),
             whole((cols, out_cols)),
-            whole(query.shape),
-            whole(rotary_q.shape),
+            whole(q_nope.shape),
+            whole(q_rope.shape),
             pl.BlockSpec((1, rows, LANES), lambda b: (b, 0, 0)),
         ],
         out_specs=(
             pl.BlockSpec((rows, out_cols), lambda b: (b, 0)),
             pl.BlockSpec((rows, out_cols), lambda b: (b, 0)),
+            pl.BlockSpec((ROPE, rows), lambda b: (0, b)),
             whole((1, out_cols)),
         ),
         scratch_shapes=[
             pltpu.VMEM((n_blocks, heads, rows), jnp.float32),
             pltpu.VMEM((n_blocks, rows, out_cols), jnp.bfloat16),
         ],
-    )(latent, kv_gain, w_up_key, w_up_value, query, rotary_q, rope)
+    )(latent, kv_gain, w_up_key, w_up_value, q_nope, q_rope, rope)
 
 
 def local(
     tokens, offsets, in_gain, w_latent, w_rope_key, kv_gain, w_up_key, w_up_value, q_nope, q_rope
 ):
-    prompts, rows, _ = tokens.shape
-    block = lax.axis_index("sp")
-    half = ROPE // 2
-    position = offsets[:, None] + block * rows + jnp.arange(rows, dtype=jnp.int32)[None, :]
-    inverse = 10000.0 ** (-jnp.arange(0, ROPE, 2).astype(jnp.float32) / ROPE)
-    angle = position.reshape(-1).astype(jnp.float32)[:, None] * inverse
-    pad = ((0, 0), (0, LANES - ROPE))
-    cosine, sine = jnp.cos(angle), jnp.sin(angle)
-    cosine = jnp.pad(jnp.concatenate([cosine, cosine], axis=1), pad)
-    sine = jnp.pad(jnp.concatenate([-sine, sine], axis=1), pad)
-    w_rope = jnp.concatenate([w_rope_key, w_rope_key[:, half:], w_rope_key[:, :half]], axis=1)
-    w_rope = jnp.pad(w_rope, ((0, 0), (0, LANES - 2 * ROPE)))
-    latent, rope = gather_latent(tokens, w_latent, w_rope, in_gain[None], cosine, sine)
-
-    heads = w_up_key.shape[1] // HEAD
-    eye = jnp.eye(heads, dtype=q_nope.dtype)
-    query = (eye[:, :, None] * q_nope.reshape(1, heads, HEAD)).reshape(heads, heads * HEAD)
-    rotary_q = jnp.pad(q_rope.reshape(heads, ROPE), pad)
-    keys, values, read = fill_cache(
-        latent, kv_gain[None], w_up_key, w_up_value, query, rotary_q, rope
+    frequency = np.float32(10000.0) ** (-np.arange(0, ROPE, 2).astype(np.float32) / ROPE)
+    inverse = np.zeros((1, LANES), np.float32)
+    inverse[0, :ROPE] = np.concatenate([frequency, frequency])
+    inverse = jnp.asarray(inverse)
+    latent, rope = gather_latent(tokens, w_latent, w_rope_key.T, in_gain[None], offsets, inverse)
+    keys, values, rope_keys, read = fill_cache(
+        latent, kv_gain[None], w_up_key, w_up_value, q_nope, q_rope, rope
     )
-    rope_keys = rope.reshape(-1, LANES)[:, :ROPE].T
     return (keys[None], values[None], rope_keys[None], read)
 
 

time: 106 us -> 84.2 us (0.79)
  Pallas kernels: 94.4 us -> 82.6 us
  local copies, waits for them, and re-layouts: 5.54 us -> 0 us
  other arithmetic: 4.31 us -> 0 us
    pallas_call x1, Pallas kernels: 87.3 us -> 75.7 us  [gather_latent(): pl.pallas_call(functools.partial(gather_kernel, n_grp, n_sp, n_tp, groups...]
    concatenate x2 -> x0, other arithmetic: 2.13 us -> none  [the longest x1 2.13 us: local(): jnp.concatenate([w_rope_key, w_rope_key[:, half:], w_rope_key[:, :half]],...]
    slice x3 -> x0, local copies, waits for them, and re-layouts: 1.94 us -> none  [the longest x2 1.46 us: local(): w_rope_key[:, half:]]
    pad x3 -> x0, local copies, waits for them, and re-layouts: 1.91 us -> none  [the longest x1 0.67 us: local(): cosine = jnp.pad(jnp.concatenate([cosine, cosine], axis=1), pad)]
    unnamed x2 -> x0, other arithmetic: 1.4 us -> none
    unnamed x6 -> x0, local copies, waits for them, and re-layouts: 1.24 us -> none
where the time goes in v2:
time: 84.2 us; the launch traced here: 83.9 us
  Pallas kernels  82.6 us (98%)
  between operations  1.28 us (2%)
    pallas_call x1, Pallas kernels, gather_latent(): pl.pallas_call(functools.partial(gather_kernel, n_grp, n_sp, n_tp, groups...  75.7 us
    pallas_call x1, Pallas kernels, fill_cache(): pl.pallas_call(functools.partial(cache_kernel, n_blocks), grid=(n_blocks,...  6.95 us

profile of v2, /device:TPU:3, one launch (start us, length us, event | category | flops | bytes accessed | tf_op | source)
XLA Modules:
  0.0 83.9 jit_solution(12474305330997347052)
XLA Ops:
  1.3 75.7 %shard_map.138 = (bf16[4,256,1024]{2,1,0:T(8,128)(2,1)}, bf16[4,256,128]{2,1,0:T(8,128)(2,1)}) custom-call(bf16[256,4096]{1,0:T(8,128)(2,1)} %bitcast.7, bf16[1024,1024]{1,0:T(8,128)(2,1)} %w_hbm.1, bf16[32,4096]{1,0:T(8,128)(2,1)} %bitcast.8, f32[1,4096]{1,0:T(1,128)} %bitcast.9, s32[1]{0:T(128)S(6)} %copy.15.offsets, f32[1,128]{1,0:T(1,128)} %constant.2.clone.inverse), custom_call_target="tpu_custom_call" | custom-call | tf_op jit(solution)/shard_map/pallas_call | solution.py:397
  77.0 7.0 %shard_map.139 = (bf16[1024,512]{1,0:T(8,128)(2,1)}, bf16[1024,512]{1,0:T(8,128)(2,1)}, bf16[32,1024]{1,0:T(8,128)(2,1)}, bf16[1,512]{1,0:T(2,128)(2,1)}) custom-call(bf16[4,256,1024]{2,1,0:T(8,128)(2,1)} %get-tuple-element.10.latent_ref, f32[1,1024]{1,0:T(1,128)} %bitcast.10, bf16[1024,512]{1,0:T(8,128)(2,1)} %wk_ref.1, bf16[1024,512]{1,0:T(8,128)(2,1)} %wv_ref.1, ...), custom_call_target="tpu_custom_call" | custom-call | tf_op jit(solution)/shard_map/pallas_call | solution.py:509

commit v3 on v2

--- a/solution.py
+++ b/solution.py
@@ -44,6 +44,7 @@
     own_rope,
     transit,
     local_sem,
+    own_send,
     z_send,
     z_recv,
     a_send,
@@ -110,21 +111,46 @@
         remote(ref, ref, recv, recv, tp_of(x, 1 - core)).wait_recv()
 
     units = [(g, d) for g in range(groups) for d in range(1, n_sp)]
-
-    def stage_z(u):
+    above = n_sp - 1 - z
+    both = jnp.minimum(z, above)
+
+    def shard(d):
+        paired = d <= 2 * both
+        hop = jnp.where(paired, (d + 1) // 2, d - both)
+        up = jnp.where(paired, d % 2 == 1, above > z)
+        return jnp.where(up, z + hop, z - hop), up
+
+    shards = {d: shard(d) for d in range(1, n_sp)}
+
+    def own_z(g):
+        for side, ahead, exists in ((0, z + 1, z + 1 < n_sp), (1, z + n_sp - 1, z > 0)):
+            copy = remote(
+                w_hbm.at[pl.ds(rank * chunk, chunk), pl.ds(g * width, width)],
+                wbuf.at[g, z, core, x, y],
+                own_send.at[g, side],
+                z_recv.at[g, z],
+                {"sp": lax.rem(ahead, n_sp)},
+            )
+            pl.when(exists)(copy.start)
+            finish.append(lambda exists=exists, copy=copy: pl.when(exists)(copy.wait_send))
+
+    def pass_z(u):
         g, d = units[u]
+        s, up = shards[d]
+        exists = jnp.where(up, z > 0, z + 1 < n_sp)
+        ahead = jnp.where(up, z + n_sp - 1, z + 1)
         copy = remote(
-            w_hbm.at[pl.ds(rank * chunk, chunk), pl.ds(g * width, width)],
-            wbuf.at[g, d - 1, core, x, y],
+            block_a(u),
+            block_a(u),
             z_send.at[u],
-            z_recv.at[u],
-            {"sp": lax.rem(z + n_sp - d, n_sp)},
+            z_recv.at[g, s],
+            {"sp": lax.rem(ahead, n_sp)},
         )
-        copy.start()
-        finish.append(copy.wait_send)
+        pl.when(exists)(copy.start)
+        finish.append(lambda: pl.when(exists)(copy.wait_send))
 
     def x_first(u):
-        return u % 2 == 1
+        return u % 3 > 0
 
     def spread(u, src, send, recv, along_x):
         peers = x_peers if along_x else y_peers
@@ -141,16 +167,17 @@
 
     def block_a(u):
         g, d = units[u]
-        return wbuf.at[g, d - 1, core, x, y]
+        return wbuf.at[g, shards[d][0], core, x, y]
 
     def block_b(u):
         g, d = units[u]
         if x_first(u):
-            return wbuf.at[g, d - 1, core, :, y]
-        return wbuf.at[g, d - 1, core, x]
+            return wbuf.at[g, shards[d][0], core, :, y]
+        return wbuf.at[g, shards[d][0], core, x]
 
     def stage_a(u):
-        arrived(block_a(u), z_recv.at[u])
+        arrived(block_a(u), z_recv.at[units[u][0], shards[units[u][1]][0]])
+        pass_z(u)
         spread(u, block_a(u), a_send, a_recv, x_first(u))
 
     def stage_b(u):
@@ -163,17 +190,18 @@
         g, d = units[u]
         for k in range(len(y_peers if x_first(u) else x_peers)):
             arrived(block_b(u), b_recv.at[u, k])
-        ref = wbuf.at[g, d - 1, core]
+        ref = wbuf.at[g, shards[d][0], core]
         copy = remote(ref, ref, c_send.at[u], c_recv.at[u], tp_of(x, 1 - core))
         copy.start()
         finish.append(copy.wait_send)
 
     def stage_dot(u):
         g, d = units[u]
-        arrived(wbuf.at[g, d - 1, core], c_recv.at[u])
-        weight = wbuf[g, d - 1].reshape(depth, width)
+        arrived(wbuf.at[g, shards[d][0], core], c_recv.at[u])
+        s, _ = shards[d]
+        weight = wbuf[g, s].reshape(depth, width)
         acc[g] += jnp.dot(
-            normed[lax.rem(z + d, n_sp)], weight, preferred_element_type=jnp.float32
+            normed[s], weight, preferred_element_type=jnp.float32
         )
 
     def crossing(m):
@@ -281,8 +309,8 @@
 
             pl.when(t * prompts + i == z)(keep)
 
-    for u in range(len(units)):
-        stage_z(u)
+    for g in range(groups):
+        own_z(g)
 
     step_rows, pieces = 16, 4
 
@@ -407,14 +435,15 @@
             pltpu.VMEM((depth, cols), bf16),
             pltpu.VMEM((ROPE, width), bf16),
             pltpu.VMEM((n_sp, total, depth), bf16),
-            pltpu.VMEM((groups, n_sp - 1, CORES, n_x, n_grp, chunk, part), bf16),
+            pltpu.VMEM((groups, n_sp, CORES, n_x, n_grp, chunk, part), bf16),
             pltpu.VMEM((groups, total, part), f32),
             pltpu.VMEM((groups, prompts, rows, part), bf16),
             pltpu.VMEM((prompts, rows, LANES), bf16),
             pltpu.VMEM((items, prompts, rows, part), bf16),
             dma((3,)),
+            dma((groups, 2)),
             dma((units,)),
-            dma((units,)),
+            dma((groups, n_sp)),
             dma((units, peers)),
             dma((units, peers)),
             dma((units, peers)),

time: 84.2 us -> 78.4 us (0.931)
  Pallas kernels: 82.6 us -> 76.8 us
    pallas_call x1, Pallas kernels: 75.7 us -> 69.8 us  [gather_latent(): pl.pallas_call(functools.partial(gather_kernel, n_grp, n_sp, n_tp, groups...]
where the time goes in v3:
time: 78.4 us; the launch traced here: 78.1 us
  Pallas kernels  76.8 us (98%)
  between operations  1.28 us (2%)
    pallas_call x1, Pallas kernels, gather_latent(): pl.pallas_call(functools.partial(gather_kernel, n_grp, n_sp, n_tp, groups...  69.8 us
    pallas_call x1, Pallas kernels, fill_cache(): pl.pallas_call(functools.partial(cache_kernel, n_blocks), grid=(n_blocks,...  6.95 us

profile of v3, /device:TPU:3, one launch (start us, length us, event | category | flops | bytes accessed | tf_op | source)
XLA Modules:
  0.0 78.1 jit_solution(17163572744357528714)
XLA Ops:
  1.3 69.8 %shard_map.138 = (bf16[4,256,1024]{2,1,0:T(8,128)(2,1)}, bf16[4,256,128]{2,1,0:T(8,128)(2,1)}) custom-call(bf16[256,4096]{1,0:T(8,128)(2,1)} %bitcast.7, bf16[1024,1024]{1,0:T(8,128)(2,1)} %w_hbm.1, bf16[32,4096]{1,0:T(8,128)(2,1)} %bitcast.8, f32[1,4096]{1,0:T(1,128)} %bitcast.9, s32[1]{0:T(128)S(6)} %copy.15.offsets, f32[1,128]{1,0:T(1,128)} %constant.2.clone.inverse), custom_call_target="tpu_custom_call" | custom-call | tf_op jit(solution)/shard_map/pallas_call | solution.py:425
  71.1 6.9 %shard_map.139 = (bf16[1024,512]{1,0:T(8,128)(2,1)}, bf16[1024,512]{1,0:T(8,128)(2,1)}, bf16[32,1024]{1,0:T(8,128)(2,1)}, bf16[1,512]{1,0:T(2,128)(2,1)}) custom-call(bf16[4,256,1024]{2,1,0:T(8,128)(2,1)} %get-tuple-element.10.latent_ref, f32[1,1024]{1,0:T(1,128)} %bitcast.10, bf16[1024,512]{1,0:T(8,128)(2,1)} %wk_ref.1, bf16[1024,512]{1,0:T(8,128)(2,1)} %wv_ref.1, ...), custom_call_target="tpu_custom_call" | custom-call | tf_op jit(solution)/shard_map/pallas_call | solution.py:538

commit v4 on v3

--- a/solution.py
+++ b/solution.py
@@ -205,12 +205,12 @@
         )
 
     def crossing(m):
-        return m % 2 == 0 and m > 0 and m < groups and n_x % 2 == 0
+        return m % 2 == 1 and m < groups and n_x % 2 == 0
 
     def slot(m, s):
         if m == 0:
             return rope_out.at[s]
-        return lat_out.at[s, :, pl.ds((m - 1) * width, width)]
+        return lat_out.at[m - 1, s]
 
     def mine(m, i):
         return own_rope.at[i] if m == 0 else own.at[m - 1, i]
@@ -425,7 +425,7 @@
     return pl.pallas_call(
         functools.partial(gather_kernel, n_grp, n_sp, n_tp, groups),
         out_shape=(
-            jax.ShapeDtypeStruct((n_sp, rows, cols), bf16),
+            jax.ShapeDtypeStruct((groups, n_sp, rows, part), bf16),
             jax.ShapeDtypeStruct((n_sp, rows, LANES), bf16),
         ),
         in_specs=[hbm, hbm, hbm, vmem, pl.BlockSpec(memory_space=pltpu.SMEM), vmem],
@@ -498,7 +498,8 @@
         jnp.where(fold, 1.0, 0.0).astype(jnp.bfloat16),
         preferred_element_type=jnp.float32,
     ).astype(jnp.bfloat16)
-    raw = latent_ref[0].astype(jnp.float32)
+    parts = [latent_ref[g, 0] for g in range(latent_ref.shape[0])]
+    raw = jnp.concatenate(parts, axis=1).astype(jnp.float32)
     scale = lax.rsqrt(jnp.mean(raw * raw, axis=-1, keepdims=True) + EPS)
     latent = (raw * scale * gain_ref[...]).astype(jnp.bfloat16)
     keys = jnp.dot(latent, wk_ref[...], preferred_element_type=jnp.float32).astype(jnp.bfloat16)
@@ -530,7 +531,8 @@
 
 
 def fill_cache(latent, kv_gain, w_up_key, w_up_value, q_nope, q_rope, rope):
-    n_blocks, rows, cols = latent.shape
+    groups, n_blocks, rows, part = latent.shape
+    cols = groups * part
     out_cols = w_up_key.shape[1]
     heads = out_cols // HEAD
     length = n_blocks * rows
@@ -545,7 +547,7 @@
             jax.ShapeDtypeStruct((1, out_cols), jnp.bfloat16),
         ),
         in_specs=[
-            pl.BlockSpec((1, rows, cols), lambda b: (b, 0, 0)),
+            pl.BlockSpec((groups, 1, rows, part), lambda b: (0, b, 0, 0)),
             whole((1, cols)),
             whole((cols, out_cols)),
             whole((cols, out_cols)),

time: 78.4 us -> 75.8 us (0.967)
  Pallas kernels: 76.8 us -> 74 us
    pallas_call x1, Pallas kernels: 69.8 us -> 67.1 us  [gather_latent(): pl.pallas_call(functools.partial(gather_kernel, n_grp, n_sp, n_tp, groups...]
where the time goes in v4:
time: 75.8 us; the launch traced here: 75.3 us
  Pallas kernels  74 us (98%)
  between operations  1.28 us (2%)
    pallas_call x1, Pallas kernels, gather_latent(): pl.pallas_call(functools.partial(gather_kernel, n_grp, n_sp, n_tp, groups...  67.1 us
    pallas_call x1, Pallas kernels, fill_cache(): pl.pallas_call(functools.partial(cache_kernel, n_blocks), grid=(n_blocks,...  6.9 us

profile of v4, /device:TPU:3, one launch (start us, length us, event | category | flops | bytes accessed | tf_op | source)
XLA Modules:
  0.0 75.3 jit_solution(15425152097355622238)
XLA Ops:
  1.3 67.1 %shard_map.138 = (bf16[4,4,256,256]{3,2,1,0:T(8,128)(2,1)}, bf16[4,256,128]{2,1,0:T(8,128)(2,1)}) custom-call(bf16[256,4096]{1,0:T(8,128)(2,1)} %bitcast.7, bf16[1024,1024]{1,0:T(8,128)(2,1)} %w_hbm.1, bf16[32,4096]{1,0:T(8,128)(2,1)} %bitcast.8, f32[1,4096]{1,0:T(1,128)} %bitcast.9, s32[1]{0:T(128)S(6)} %copy.15.offsets, f32[1,128]{1,0:T(1,128)} %constant.2.clone.inverse), custom_call_target="tpu_custom_call" | custom-call | tf_op jit(solution)/shard_map/pallas_call | solution.py:425
  68.4 6.9 %shard_map.139 = (bf16[1024,512]{1,0:T(8,128)(2,1)}, bf16[1024,512]{1,0:T(8,128)(2,1)}, bf16[32,1024]{1,0:T(8,128)(2,1)}, bf16[1,512]{1,0:T(2,128)(2,1)}) custom-call(bf16[4,4,256,256]{3,2,1,0:T(8,128)(2,1)} %get-tuple-element.10.latent_ref, f32[1,1024]{1,0:T(1,128)} %bitcast.10, bf16[1024,512]{1,0:T(8,128)(2,1)} %wk_ref.1, bf16[1024,512]{1,0:T(8,128)(2,1)} %wv_ref.1, ...), custom_call_target="tpu_custom_call" | custom-call | tf_op jit(solution)/shard_map/pallas_call | solution.py:540
